TPU v7x, 32 devices: a whole 2x2x4 slice. The times are simulated.
32 devices in a mesh: sp: 16 (over z, y, x), tp: 2 (over core).
Axes of the slice: x: 2, y: 2, z: 4, core: 2. Of those that a mesh axis runs over, the one named last changes fastest.
Arguments:
- tokens: bfloat16 [4096, 2048], P(('sp', 'tp')), may hold values from -6 to 6
- documents: int32 [4096], P('sp'), may hold values from 0 to 3, never falling along the last dimension, each value on 1 to 2048 neighbouring positions
- w_query: bfloat16 [2, 2048, 512], P(None, None, 'tp'), may hold values from -0.125 to 0.125
- w_key: bfloat16 [2, 2048, 256], P(None, None, 'tp'), may hold values from -0.125 to 0.125
- w_value: bfloat16 [2, 2048, 256], P(None, None, 'tp'), may hold values from -0.125 to 0.125
- w_out: bfloat16 [2, 512, 2048], P(None, 'tp'), may hold values from -0.25 to 0.25
- rel_table: float32 [2, 8, 257], P(None, 'tp'), may hold values from -250 to 250
- norm_gain: float32 [2, 2048], replicated, may hold values from 0.1 to 1.9
- norm_shift: float32 [2, 2048], replicated, may hold values from -3 to 3
Outputs:
- encoded: bfloat16 [4096, 2048], P(('sp', 'tp'))
Inputs may be any that keep to these rules, and one draw needn't show every extreme that they name: `documents`: document numbers never fall along the sequence; a document spans at most 2048 positions.
All inputs are finite; a program needn't handle non-finite values.
Results may differ from a plain program's by a relative error of at most 0.0075.
Values may be sent and summed in bfloat16 or wider, within the bound.
A program may use at most 64 MiB of HBM per device.

v0:
```python
import functools

import jax
import jax.numpy as jnp
from jax import lax
from jax.experimental import pallas as pl
from jax.experimental.pallas import tpu as pltpu
from jax.sharding import PartitionSpec as P

HD = 64
SEG = 64
LEFT = 4
CLIP = 128
MESH = pl.DeviceIdType.MESH
F32 = jnp.float32
BF16 = jnp.bfloat16


def kernel(n_sp, tok_h, doc_h, wq_h, wk_h, wv_h, wo_h, tbl_h, gain_h, shift_h, out,
           x, res, wq, wkv, wo, tbl, gain, shift, doc_own, doc_prev, kv, qst, bias, att, stat, begun,
           loc_sem, w_send, w_recv, s_send, s_recv, kv_send, kv_recv, out_sem):
    sp = lax.axis_index("sp")
    tp = lax.axis_index("tp")
    other = 1 - tp
    layers = wq.shape[0]
    rows = x.shape[0]
    has_next = sp < n_sp - 1
    has_prev = sp > 0
    scale_res = (2.0 * layers) ** 0.25

    def local(src, dst, i):
        copy = pltpu.make_async_copy(src, dst, loc_sem.at[i])
        copy.start()
        return copy

    c_wkv, c_wq, c_wo = [], [], []
    for l in range(layers):
        base = 6 + 4 * l
        if l == 0:
            c_x = local(tok_h, x, 0)
        c_wkv.append((local(wk_h.at[l], wkv.at[l, tp, :, 0:2 * HD], base),
                      local(wv_h.at[l], wkv.at[l, tp, :, 2 * HD:4 * HD], base + 1)))
        if l == 0:
            c_doc = local(doc_h, doc_own, 1)
            c_tbl = local(tbl_h, tbl.at[tp], 2)
        c_wq.append(local(wq_h.at[l], wq.at[l, tp], base + 2))
        c_wo.append(local(wo_h.at[l], wo.at[l, tp], base + 3))
        if l == 0:
            c_gain = local(gain_h, gain, 3)
            c_shift = local(shift_h, shift, 4)

    barrier = pltpu.get_barrier_semaphore()

    def greet(dev_sp, dev_tp):
        pl.semaphore_signal(barrier, inc=1, device_id=(dev_sp, dev_tp), device_id_type=MESH)

    greet(sp, other)

    @pl.when(has_prev)
    def _():
        greet(sp - 1, tp)

    @pl.when(jnp.logical_not(has_prev))
    def _():
        doc_prev[...] = jnp.full_like(doc_prev, -1)
        for l in range(layers):
            for h in range(2):
                kv[l, h, 0:rows, :] = jnp.zeros((rows, 4 * HD), BF16)

        @pl.when(tp == 0)
        def _():
            for l in range(layers):
                for h in range(2):
                    kv[l, h, rows:2 * rows, :] = jnp.zeros((rows, 4 * HD), BF16)

    pl.semaphore_wait(barrier, jnp.where(has_next, 2, 1))

    def wcopy(ref, l, kind, half):
        return pltpu.make_async_remote_copy(
            src_ref=ref.at[l, half], dst_ref=ref.at[l, half],
            send_sem=w_send.at[l, kind], recv_sem=w_recv.at[l, kind],
            device_id=(sp, other), device_id_type=MESH)

    def send_w(ref, l, kind):
        wcopy(ref, l, kind, tp).start()

    def await_w(ref, l, kind):
        wcopy(ref, l, kind, other).wait_recv()

    def tbl_copy(half):
        return pltpu.make_async_remote_copy(
            src_ref=tbl.at[half], dst_ref=tbl.at[half], send_sem=s_send.at[0], recv_sem=s_recv.at[0],
            device_id=(sp, other), device_id_type=MESH)

    def doc_copy():
        return pltpu.make_async_remote_copy(
            src_ref=doc_own, dst_ref=doc_prev, send_sem=s_send.at[1], recv_sem=s_recv.at[1],
            device_id=(sp + 1, tp), device_id_type=MESH)

    def block(l, half, slot):
        return kv.at[l, half, pl.ds(slot * rows, rows), :]

    def kv_copy(l, half, src, slot, dev_sp, dev_tp):
        return pltpu.make_async_remote_copy(
            src_ref=block(l, half, src), dst_ref=block(l, half, slot),
            send_sem=kv_send.at[l, half, slot], recv_sem=kv_recv.at[l, half, slot],
            device_id=(dev_sp, dev_tp), device_id_type=MESH)

    def send_kv(l, half):
        @pl.when(has_next)
        def _():
            kv_copy(l, half, 2, 0, sp + 1, tp).start()

        @pl.when(tp == 0)
        def _():
            kv_copy(l, half, 2, 1, sp, 1).start()

    def await_kv(l, half):
        @pl.when(has_prev)
        def _():
            kv_copy(l, half, 2, 0, sp, other).wait_recv()

            @pl.when(tp == 1)
            def _():
                kv_copy(l, half, 0, 1, sp, 0).start()

        @pl.when((tp == 1) | has_prev)
        def _():
            kv_copy(l, half, 2, 1, sp, other).wait_recv()

    def await_sent_kv(l, half):
        @pl.when(has_next)
        def _():
            kv_copy(l, half, 2, 0, sp, other).wait_send()

        @pl.when((tp == 0) | has_prev)
        def _():
            kv_copy(l, half, 2, 1, sp, other).wait_send()

    def make_kv(l, half):
        y = jnp.dot(x[...], wkv[l, half], preferred_element_type=F32)
        kv[l, half, 2 * rows:3 * rows, :] = y.astype(BF16)

    lane = lax.broadcasted_iota(jnp.int32, (rows, 2 * HD), 1)
    low = lane < HD

    def make_q(l, half):
        y = jnp.dot(x[...], wq[l, half], preferred_element_type=F32)
        y = y.astype(BF16).astype(F32) * (HD ** -0.5)
        for j in range(2):
            pair = y[:, 2 * HD * j:2 * HD * (j + 1)]
            turned = pltpu.roll(pair, HD, 1)
            if j == 0:
                first, second = jnp.where(low, pair, 0.0), jnp.where(low, turned, 0.0)
            else:
                first, second = jnp.where(low, 0.0, turned), jnp.where(low, 0.0, pair)
            qst[2 * half + j, 0:rows, :] = first.astype(BF16)
            qst[2 * half + j, rows:2 * rows, :] = second.astype(BF16)

    def make_bias():
        first = tp == 0
        dp = doc_prev[...].astype(F32)
        do = doc_own[...].astype(F32)
        k0 = jnp.where(first, dp[0:1], dp[1:2])
        k1 = jnp.where(first, dp[1:2], do[0:1])
        k2 = jnp.where(first, do[0:1], do[1:2])
        e = lax.broadcasted_iota(jnp.int32, (rows, rows), 0)
        r = lax.broadcasted_iota(jnp.int32, (rows, rows), 1)
        shape = (rows, rows)
        queries = jnp.broadcast_to(k2, shape)
        same = [jnp.broadcast_to(k, shape).T == queries for k in (k0, k1, k2)]
        valid = [same[0] & ((e >= SEG) | (r < SEG)), same[1], same[2] & ((e < SEG) | (r >= SEG))]
        for l in range(layers):
            for head in range(8):
                half, i = head // 4, head % 4
                t0 = jnp.broadcast_to(tbl[half, l, i:i + 1, 0:CLIP], shape)
                t1 = jnp.broadcast_to(tbl[half, l, i:i + 1, CLIP:2 * CLIP], shape)
                c = jnp.broadcast_to(tbl[half, l, i:i + 1, 2 * CLIP:2 * CLIP + 1], shape)
                b1 = pltpu.roll(jnp.concatenate([c, t1], axis=1), 0, 1, stride=1, stride_axis=0)[:, :rows]
                b2 = pltpu.roll(jnp.concatenate([t1, t0], axis=1), 0, 1, stride=1, stride_axis=0)[:, :rows]
                cols = slice((head % 2) * rows, (head % 2 + 1) * rows)
                for k, b in enumerate((c, b1, b2)):
                    bias[l, head // 2, k * rows:(k + 1) * rows, cols] = jnp.where(valid[k], b, -1e30)

    def part(l, half, j, keys):
        s = lax.dot_general(kv[l, half, keys, 0:2 * HD], qst[2 * half + j], (((1,), (1,)), ((), ())),
                            preferred_element_type=F32)
        return s + bias[l, 2 * half + j, keys, :]

    def weigh(l, half, j, keys, p):
        o = lax.dot_general(kv[l, half, keys, 2 * HD:4 * HD], p.astype(BF16), (((0,), (0,)), ((), ())),
                            preferred_element_type=F32)
        return o[HD * j:HD * (j + 1), :]

    near, far = slice(2 * rows, 3 * rows), slice(0, 2 * rows)

    def attend_own(l, half):
        for j in range(2):
            g = 2 * half + j
            s = part(l, half, j, near)
            peak = jnp.max(s, axis=0, keepdims=True)
            p = jnp.exp(s - peak)
            stat[g, 0:1, :] = peak
            stat[g, 1:2, :] = jnp.sum(p, axis=0, keepdims=True)
            begun[g] = weigh(l, half, j, near, p)

    def attend(l, half):
        for j in range(2):
            g = 2 * half + j
            s = part(l, half, j, far)
            before = stat[g, 0:1, :]
            peak = jnp.maximum(jnp.max(s, axis=0, keepdims=True), before)
            fade = jnp.exp(before - peak)
            p = jnp.exp(s - peak)
            total = jnp.sum(p, axis=0, keepdims=True) + fade * stat[g, 1:2, :]
            o = (weigh(l, half, j, far, p) + fade * begun[g]) / total
            both = jnp.concatenate([o[:, 0:rows], o[:, rows:2 * rows]], axis=0)
            att[:, 2 * HD * g:2 * HD * (g + 1)] = both.T.astype(BF16)

    width = x.shape[1]
    step = 256

    def project(l):
        a = att[...]
        kd = wo.shape[2]

        def body(i, _):
            cols = pl.ds(pl.multiple_of(i * step, step), step)
            y = jnp.dot(a[:, 0:kd], wo[l, 0, :, cols], preferred_element_type=F32)
            y = y + jnp.dot(a[:, kd:2 * kd], wo[l, 1, :, cols], preferred_element_type=F32)
            res[:, cols] = scale_res * x[:, cols].astype(F32) + y
            return 0

        lax.fori_loop(0, width // step, body, 0, unroll=True)

    def normalise(l, low_row, high_row):
        def body(i, _):
            rr = pl.ds(pl.multiple_of(i * 16, 16), 16)
            y = res[rr, :]
            mean = jnp.mean(y, axis=-1, keepdims=True)
            y = y - mean
            var = jnp.mean(y * y, axis=-1, keepdims=True)
            y = y * lax.rsqrt(var + 1e-5) * gain[l:l + 1, :] + shift[l:l + 1, :]
            x[rr, :] = y.astype(BF16)
            return 0

        lax.fori_loop(low_row // 16, high_row // 16, body, 0, unroll=2)

    c_wkv[0][0].wait()
    c_wkv[0][1].wait()
    send_w(wkv, 0, 0)
    c_doc.wait()

    @pl.when(has_next)
    def _():
        doc_copy().start()

    c_tbl.wait()
    tbl_copy(tp).start()
    c_x.wait()
    make_kv(0, tp)
    c_wq[0].wait()
    send_w(wq, 0, 1)
    send_kv(0, tp)
    make_q(0, tp)
    await_w(wkv, 0, 0)
    make_kv(0, other)
    c_wo[0].wait()
    send_w(wo, 0, 2)
    send_kv(0, other)
    for l in range(1, layers):
        c_wkv[l][0].wait()
        c_wkv[l][1].wait()
        send_w(wkv, l, 0)
        c_wq[l].wait()
        send_w(wq, l, 1)
        c_wo[l].wait()
        send_w(wo, l, 2)
    tbl_copy(other).wait_recv()

    @pl.when(has_prev)
    def _():
        doc_copy().wait_recv()

    make_bias()
    await_w(wq, 0, 1)
    make_q(0, other)
    c_gain.wait()
    c_shift.wait()
    for l in range(layers):
        if l > 0:
            await_w(wkv, l, 0)
            await_w(wq, l, 1)

            @pl.when(tp == 0)
            def _():
                make_q(l, 0)

            make_kv(l, 0)
            send_kv(l, 0)
            make_kv(l, 1)
            send_kv(l, 1)
            make_q(l, 1)

            @pl.when(tp == 1)
            def _():
                make_q(l, 0)

        attend_own(l, 0)
        attend_own(l, 1)
        for h in ((1, 0) if l == 0 else (0, 1)):
            await_kv(l, h)
            attend(l, h)
        await_w(wo, l, 2)
        project(l)
        if l < layers - 1:
            normalise(l, 0, rows)

    leaving = []
    for i in range(2):
        normalise(layers - 1, i * rows // 2, (i + 1) * rows // 2)
        part_rows = pl.ds(i * rows // 2, rows // 2)
        leaving.append(pltpu.make_async_copy(x.at[part_rows], out.at[part_rows], out_sem.at[i]))
        leaving[-1].start()

    for l in range(layers):
        for kind, ref in enumerate((wkv, wq, wo)):
            wcopy(ref, l, kind, tp).wait_send()
        for h in range(2):
            await_sent_kv(l, h)
    tbl_copy(tp).wait_send()
    for copy in leaving:
        copy.wait()

    @pl.when(has_next)
    def _():
        doc_copy().wait_send()


def solution(mesh):
    n_sp = mesh.shape["sp"]

    def shards(tokens, documents, w_query, w_key, w_value, w_out, rel_table, norm_gain, norm_shift):
        rows, width = tokens.shape
        layers = w_query.shape[0]
        docs = documents.reshape(2, rows)
        anywhere = pl.BlockSpec(memory_space=pl.ANY)
        return pl.pallas_call(
            functools.partial(kernel, n_sp),
            out_shape=jax.ShapeDtypeStruct((rows, width), BF16),
            in_specs=[anywhere] * 9,
            out_specs=anywhere,
            scratch_shapes=[
                pltpu.VMEM((rows, width), BF16),
                pltpu.VMEM((rows, width), F32),
                pltpu.VMEM((layers, 2, width, w_query.shape[2]), BF16),
                pltpu.VMEM((layers, 2, width, 2 * w_key.shape[2]), BF16),
                pltpu.VMEM((layers, 2, w_out.shape[1], width), BF16),
                pltpu.VMEM((2,) + rel_table.shape, F32),
                pltpu.VMEM((layers, width), F32),
                pltpu.VMEM((layers, width), F32),
                pltpu.VMEM((2, rows), jnp.int32),
                pltpu.VMEM((2, rows), jnp.int32),
                pltpu.VMEM((layers, 2, 3 * rows, 4 * HD), BF16),
                pltpu.VMEM((4, 2 * rows, 2 * HD), BF16),
                pltpu.VMEM((layers, 4, 3 * rows, 2 * rows), F32),
                pltpu.VMEM((rows, 2 * w_out.shape[1]), BF16),
                pltpu.VMEM((4, 8, 2 * rows), F32),
                pltpu.VMEM((4, HD, 2 * rows), F32),
                pltpu.SemaphoreType.DMA((6 + 4 * layers,)),
                pltpu.SemaphoreType.DMA((layers, 3)),
                pltpu.SemaphoreType.DMA((layers, 3)),
                pltpu.SemaphoreType.DMA((2,)),
                pltpu.SemaphoreType.DMA((2,)),
                pltpu.SemaphoreType.DMA((layers, 2, 2)),
                pltpu.SemaphoreType.DMA((layers, 2, 2)),
                pltpu.SemaphoreType.DMA((2,)),
            ],
            compiler_params=pltpu.CompilerParams(
                collective_id=0, has_side_effects=True, vmem_limit_bytes=60 * 1024 * 1024
            ),
        )(tokens, docs, w_query, w_key, w_value, w_out, rel_table, norm_gain, norm_shift)

    in_specs = (
        P(("sp", "tp"), None),
        P("sp"),
        P(None, None, "tp"),
        P(None, None, "tp"),
        P(None, None, "tp"),
        P(None, "tp", None),
        P(None, "tp", None),
        P(),
        P(),
    )
    return jax.shard_map(shards, mesh=mesh, in_specs=in_specs, out_specs=P(("sp", "tp"), None), check_vma=False)
```

profile of v0, /device:TPU:24, one launch (start us, length us, event | category | flops | bytes accessed | tf_op | source)
XLA Modules:
  0.0 25.7 jit_solution(7326218572593899644)
XLA Ops:
  0.0 23.8 %shard_map.91 = bf16[128,2048]{1,0:T(8,128)(2,1)} custom-call(bf16[128,2048]{1,0:T(8,128)(2,1)} %tok_h.1, s32[2,128]{1,0:T(2,128)} %bitcast.1, bf16[2,2048,256]{2,1,0:T(8,128)(2,1)} %wq_h.1, bf16[2,2048,128]{2,1,0:T(8,128)(2,1)} %wk_h.1, bf16[2,2048,128]{2,1,0:T(8,128)(2,1)} %wv_h.1, bf16[2,256,2048]{2,1,0:T(8,128)(2,1)} %wo_h.1, f32[2,4,257]{2,1,0:T(4,128)} %tbl_h.1, ...), custom_call_target="tpu_custom_call" | custom-call | tf_op jit(solution)/shard_map/pallas_call | solution.py:348
  23.8 1.9 %copy.11 = bf16[128,2048]{1,0:T(8,128)(2,1)} copy(bf16[128,2048]{1,0:T(8,128)(2,1)} %shard_map.91) | data formatting | bytes 1048576
where the time goes:
time: 25.8 us; the launch traced here: 25.7 us
  Pallas kernels  23.8 us (92%)
  local copies, waits for them, and re-layouts  1.88 us (7%)
    pallas_call x1, Pallas kernels, shards(): pl.pallas_call(functools.partial(kernel, n_sp), out_shape=jax.ShapeDtypeS...  23.8 us
    unnamed x1, local copies, waits for them, and re-layouts  1.88 us

commit v1 on v0

--- a/solution.py
+++ b/solution.py
@@ -18,7 +18,7 @@
 
 def kernel(n_sp, tok_h, doc_h, wq_h, wk_h, wv_h, wo_h, tbl_h, gain_h, shift_h, out,
            x, res, wq, wkv, wo, tbl, gain, shift, doc_own, doc_prev, kv, qst, bias, att, stat, begun,
-           loc_sem, w_send, w_recv, s_send, s_recv, kv_send, kv_recv, out_sem):
+           loc_sem, w_send, w_recv, s_send, s_recv, kv_send, kv_recv):
     sp = lax.axis_index("sp")
     tp = lax.axis_index("tp")
     other = 1 - tp
@@ -233,7 +233,7 @@
 
         lax.fori_loop(0, width // step, body, 0, unroll=True)
 
-    def normalise(l, low_row, high_row):
+    def normalise(l, dst):
         def body(i, _):
             rr = pl.ds(pl.multiple_of(i * 16, 16), 16)
             y = res[rr, :]
@@ -241,10 +241,10 @@
             y = y - mean
             var = jnp.mean(y * y, axis=-1, keepdims=True)
             y = y * lax.rsqrt(var + 1e-5) * gain[l:l + 1, :] + shift[l:l + 1, :]
-            x[rr, :] = y.astype(BF16)
+            dst[rr, :] = y.astype(BF16)
             return 0
 
-        lax.fori_loop(low_row // 16, high_row // 16, body, 0, unroll=2)
+        lax.fori_loop(0, rows // 16, body, 0, unroll=2)
 
     c_wkv[0][0].wait()
     c_wkv[0][1].wait()
@@ -313,15 +313,7 @@
             attend(l, h)
         await_w(wo, l, 2)
         project(l)
-        if l < layers - 1:
-            normalise(l, 0, rows)
-
-    leaving = []
-    for i in range(2):
-        normalise(layers - 1, i * rows // 2, (i + 1) * rows // 2)
-        part_rows = pl.ds(i * rows // 2, rows // 2)
-        leaving.append(pltpu.make_async_copy(x.at[part_rows], out.at[part_rows], out_sem.at[i]))
-        leaving[-1].start()
+        normalise(l, x if l < layers - 1 else out)
 
     for l in range(layers):
         for kind, ref in enumerate((wkv, wq, wo)):
@@ -329,8 +321,6 @@
         for h in range(2):
             await_sent_kv(l, h)
     tbl_copy(tp).wait_send()
-    for copy in leaving:
-        copy.wait()
 
     @pl.when(has_next)
     def _():
@@ -347,9 +337,9 @@
         anywhere = pl.BlockSpec(memory_space=pl.ANY)
         return pl.pallas_call(
             functools.partial(kernel, n_sp),
-            out_shape=jax.ShapeDtypeStruct((rows, width), BF16),
+            out_shape=pltpu.VMEM((rows, width), BF16),
             in_specs=[anywhere] * 9,
-            out_specs=anywhere,
+            out_specs=pl.BlockSpec(memory_space=pltpu.VMEM),
             scratch_shapes=[
                 pltpu.VMEM((rows, width), BF16),
                 pltpu.VMEM((rows, width), F32),
@@ -374,7 +364,6 @@
                 pltpu.SemaphoreType.DMA((2,)),
                 pltpu.SemaphoreType.DMA((layers, 2, 2)),
                 pltpu.SemaphoreType.DMA((layers, 2, 2)),
-                pltpu.SemaphoreType.DMA((2,)),
             ],
             compiler_params=pltpu.CompilerParams(
                 collective_id=0, has_side_effects=True, vmem_limit_bytes=60 * 1024 * 1024

time: 25.8 us -> 24 us (0.930)
  local copies, waits for them, and re-layouts: 1.88 us -> 0.8 us
  Pallas kernels: 23.8 us -> 23.1 us
    unnamed x1, local copies, waits for them, and re-layouts: 1.88 us -> 0.8 us
    pallas_call x1, Pallas kernels: 23.8 us -> 23.1 us  [shards(): pl.pallas_call(functools.partial(kernel, n_sp), out_shape=pltpu.VMEM((row...]
where the time goes in v1:
time: 24 us; the launch traced here: 23.9 us
  Pallas kernels  23.1 us (96%)
  local copies, waits for them, and re-layouts  0.8 us (3%)
    pallas_call x1, Pallas kernels, shards(): pl.pallas_call(functools.partial(kernel, n_sp), out_shape=pltpu.VMEM((row...  23.1 us
    unnamed x1, local copies, waits for them, and re-layouts  0.8 us

profile of v1, /device:TPU:24, one launch (start us, length us, event | category | flops | bytes accessed | tf_op | source)
XLA Modules:
  0.0 23.9 jit_solution(3386730937024046629)
XLA Ops:
  0.0 23.1 %shard_map.91 = bf16[128,2048]{1,0:T(8,128)(2,1)S(1)} custom-call(bf16[128,2048]{1,0:T(8,128)(2,1)} %tok_h.1, s32[2,128]{1,0:T(2,128)} %bitcast.1, bf16[2,2048,256]{2,1,0:T(8,128)(2,1)} %wq_h.1, bf16[2,2048,128]{2,1,0:T(8,128)(2,1)} %wk_h.1, bf16[2,2048,128]{2,1,0:T(8,128)(2,1)} %wv_h.1, bf16[2,256,2048]{2,1,0:T(8,128)(2,1)} %wo_h.1, f32[2,4,257]{2,1,0:T(4,128)} %tbl_h.1, ...), custom_call_target="tpu_custom_call" | custom-call | tf_op jit(solution)/shard_map/pallas_call | solution.py:338
  23.1 0.8 %copy.11 = bf16[128,2048]{1,0:T(8,128)(2,1)} copy(bf16[128,2048]{1,0:T(8,128)(2,1)S(1)} %shard_map.91) | data formatting | bytes 1048576
